TPU v7x, 32 devices: a whole 2x2x4 slice. The times are simulated.
32 devices in a mesh: rep: 2 (over y), fs: 4 (over z), tp: 4 (over x, core).
Axes of the slice: x: 2, y: 2, z: 4, core: 2. Of those that a mesh axis runs over, the one named last changes fastest.
Arguments:
- tokens: bfloat16 [2048, 2048], P(('rep', 'fs')), may hold values from -6 to 6
- gate_weight: bfloat16 [2048, 2816], P('fs', 'tp'), may hold values from -0.125 to 0.125
- up_weight: bfloat16 [2048, 2816], P('fs', 'tp'), may hold values from -0.125 to 0.125
- down_weight: bfloat16 [2816, 2048], P('tp', 'fs'), may hold values from -0.109375 to 0.109375
- out_grad: bfloat16 [2048, 2048], P(('rep', 'fs')), may hold values from -6 to 6
Outputs:
- input_grad: bfloat16 [2048, 2048], P(('rep', 'fs'))
- down_grad: float32 [2816, 2048], P('tp', 'fs')
- row_norms: float32 [2816], P('tp')
All inputs are finite; a program needn't handle non-finite values.
Results may differ from a plain program's by a relative error of at most 0.024.
Values may be sent and summed in bfloat16 or wider, within the bound.
A program may use at most 64 MiB of HBM per device.

v0:
```python
import jax
import jax.numpy as jnp
from jax import lax
from jax.sharding import PartitionSpec as P


def contract_last(left, right):
    return lax.dot_general(
        left, right, (((1,), (1,)), ((), ())), preferred_element_type=jnp.float32
    )


def contract_first(left, right):
    return lax.dot_general(
        left, right, (((0,), (0,)), ((), ())), preferred_element_type=jnp.float32
    )


def on_device(tokens, gate_weight, up_weight, down_weight, out_grad):
    down_full = lax.all_gather(down_weight, "fs", axis=1, tiled=True)
    gate_full, up_full = (
        lax.all_gather(gate_weight, "fs", axis=0, tiled=True),
        lax.all_gather(up_weight, "fs", axis=0, tiled=True),
    )
    gate_pre = jnp.dot(tokens, gate_full, preferred_element_type=jnp.float32)
    up_pre = jnp.dot(tokens, up_full, preferred_element_type=jnp.float32)
    sigma = jax.nn.sigmoid(gate_pre)
    activated = gate_pre * sigma
    hidden = (activated * up_pre).astype(jnp.bfloat16)
    hid_grad = contract_last(out_grad, down_full)
    up_grad = (hid_grad * activated).astype(jnp.bfloat16)
    gate_grad = (hid_grad * up_pre * sigma * (1.0 + gate_pre * (1.0 - sigma))).astype(jnp.bfloat16)
    partial_value = contract_last(gate_grad, gate_full) + contract_last(up_grad, up_full)
    input_grad = lax.psum(partial_value.astype(jnp.bfloat16), "tp")
    columns = lax.all_to_all(out_grad, "fs", split_axis=1, concat_axis=0, tiled=True)
    shard = contract_first(lax.all_gather(hidden, "fs", axis=0, tiled=True), columns)
    shard = lax.psum(shard.astype(jnp.bfloat16), "rep").astype(jnp.float32)
    norms = lax.psum(jnp.sum(shard * shard, axis=1), "fs")
    return (input_grad, shard, norms)


def solution(mesh):
    return jax.shard_map(
        on_device,
        mesh=mesh,
        in_specs=(
            P(("rep", "fs"), None),
            P("fs", "tp"),
            P("fs", "tp"),
            P("tp", "fs"),
            P(("rep", "fs"), None),
        ),
        out_specs=(P(("rep", "fs"), None), P("tp", "fs"), P("tp")),
        check_vma=False,
    )
```

profile of v0, /device:TPU:0, one launch (start us, length us, event | category | flops | bytes accessed | tf_op | source)
XLA Modules:
  0.0 329.1 jit_solution(854777100918134661)
XLA Ops:
  7.2 0.7 all-gather.9.cloned.1.call-update
  8.0 0.7 all-gather.7.cloned.1.call-update
  8.7 0.7 all-gather.5.cloned.1.call-update
  9.4 0.0 all-gather.11.cloned.1.call-start
  9.4 62.0 %all-gather.9.cloned.1.call-done = bf16[2048,704]{0,1:T(8,128)(2,1)} async-done(((bf16[512,704]{0,1:T(8,128)(2,1)}), bf16[2048,704]{0,1:T(8,128)(2,1)}) %all-gather.9.cloned.1.call-update) | async-done | bytes 2883600 | tf_op jit(solution)/shard_map/all_gather | solution.py:22
  71.4 2.8 fusion.8
  74.2 56.6 %all-gather.7.cloned.1.call-done = bf16[2048,704]{0,1:T(8,128)(2,1)} async-done(((bf16[512,704]{0,1:T(8,128)(2,1)}), bf16[2048,704]{0,1:T(8,128)(2,1)}) %all-gather.7.cloned.1.call-update) | async-done | bytes 2883600 | tf_op jit(solution)/shard_map/all_gather | solution.py:23
  130.8 3.7 %multiply_convert_fusion = (bf16[256,704]{0,1:T(8,128)(2,1)}, f32[256,704]{0,1:T(8,128)}) fusion(f32[256,704]{0,1:T(8,128)S(1)} %fusion.8, bf16[256,2048]{1,0:T(8,128)(2,1)S(1)} %copy-done, bf16[2048,704]{0,1:T(8,128)(2,1)} %all-gather.7.cloned.1.call-done), kind=kOutput, calls=%fused_computation.4 | convolution fusion | flops 739278848 | bytes 5734400 | tf_op jit(solution)/shard_map/dot_general | solution.py:26
  134.6 0.0 all-reduce.5.cloned.1.call-start
  134.7 0.5 copy.8
  135.2 56.6 %all_to_all.19 = bf16[256,4,512]{0,2,1:T(8,128)(2,1)S(1)} all-to-all(bf16[256,4,512]{0,2,1:T(8,128)(2,1)S(1)} %bitcast.14), channel_id=1, replica_groups=mesh['rep'=2,'fs'=4,'tp'=4] {'fs'}, dimensions={1} | all-to-all | bytes 2097152 | tf_op jit(solution)/shard_map/all_to_all | solution.py:35
  191.8 0.5 copy.9
  192.4 17.8 %all-gather.5.cloned.1.call-done = bf16[704,2048]{1,0:T(8,128)(2,1)} async-done(((bf16[704,512]{1,0:T(8,128)(2,1)}), bf16[704,2048]{1,0:T(8,128)(2,1)}) %all-gather.5.cloned.1.call-update) | async-done | bytes 2883600 | tf_op jit(solution)/shard_map/all_gather | solution.py:20
  210.1 3.9 %fusion.7 = f32[256,704]{0,1:T(8,128)} fusion(bf16[256,2048]{1,0:T(8,128)(2,1)} %param.9, bf16[704,2048]{1,0:T(8,128)(2,1)} %all-gather.5.cloned.1.call-done), kind=kOutput, calls=%fused_computation.13 | convolution fusion | flops 738197504 | bytes 4653056 | tf_op jit(solution)/shard_map/dot_general | solution.py:8
  214.1 32.2 %all-gather.11.cloned.1.call-done = bf16[1024,704]{0,1:T(8,128)(2,1)} async-done(((bf16[256,704]{0,1:T(8,128)(2,1)}), bf16[1024,704]{0,1:T(8,128)(2,1)}) %all-gather.11.cloned.1.call-update) | async-done | bytes 1441808 | tf_op jit(solution)/shard_map/all_gather | solution.py:36
  246.3 3.2 convolution_convert_fusion
  249.5 0.0 all-reduce.3.cloned.1.call-start
  249.6 3.5 %fusion.2 = f32[256,2048]{1,0:T(8,128)S(1)} fusion(bf16[2048,704]{0,1:T(8,128)(2,1)} %all-gather.9.cloned.1.call-done, f32[256,704]{0,1:T(8,128)S(1)} %copy-done.4, f32[256,704]{0,1:T(8,128)} %fusion.7, f32[256,704]{0,1:T(8,128)} %get-tuple-element.6), kind=kOutput, calls=%fused_computation.9 | convolution fusion | flops 739999744 | bytes 7143424 | tf_op jit(solution)/shard_map/dot_general | solution.py:8
  253.1 2.0 fusion
  255.2 25.6 %all-reduce.5.cloned.1.call-done = bf16[704,512]{1,0:T(8,128)(2,1)} async-done(((bf16[704,512]{1,0:T(8,128)(2,1)}), bf16[704,512]{1,0:T(8,128)(2,1)}) %all-reduce.5.cloned.1.call-update) | async-done | bytes 720912 | tf_op jit(solution)/shard_map/psum | solution.py:37
  280.8 2.3 multiply_reduce_fusion
  283.1 12.2 %psum.23 = f32[704]{0:T(1024)} all-reduce(f32[704]{0:T(1024)S(1)} %get-tuple-element.3), channel_id=1, replica_groups=mesh['rep'=2,'fs'=4,'tp'=4] {'fs'}, use_global_device_ids=true, to_apply=%region_3.0 | all-reduce | flops 704 | bytes 5632 | tf_op jit(solution)/shard_map/psum | solution.py:38
  295.4 24.5 %all-reduce.3.cloned.1.call-done = bf16[256,2048]{1,0:T(8,128)(2,1)} async-done(((bf16[256,2048]{1,0:T(8,128)(2,1)}), bf16[256,2048]{1,0:T(8,128)(2,1)}) %all-reduce.3.cloned.1.call-update) | async-done | bytes 1048592 | tf_op jit(solution)/shard_map/psum | solution.py:34
  319.9 2.3 copy.12
  (18 shorter events, 0.2 us)
Async XLA Ops:
  7.2 64.3 %copy-start = (bf16[256,2048]{1,0:T(8,128)(2,1)S(1)}, bf16[256,2048]{1,0:T(8,128)(2,1)}, u32[]{:S(2)}) copy-start(bf16[256,2048]{1,0:T(8,128)(2,1)} %param.5) | copy-start | bytes 3145732
  7.2 64.2 %all-gather.9.cloned.1.call-start = ((), (), s32[]{:S(2)}) async-start(), calls=%async_computation.3 | async-start | bytes 3604480 | tf_op jit(solution)/shard_map/all_gather | solution.py:22
  7.9 122.9 %all-gather.7.cloned.1.call-start = ((), (), s32[]{:S(2)}) async-start(), calls=%async_computation.2 | async-start | bytes 3604480 | tf_op jit(solution)/shard_map/all_gather | solution.py:23
  8.7 201.5 %all-gather.5.cloned.1.call-start = ((), (), s32[]{:S(2)}) async-start(), calls=%async_computation.1 | async-start | bytes 3604480 | tf_op jit(solution)/shard_map/all_gather | solution.py:20
  9.4 236.9 %all-gather.11.cloned.1.call-start = ((), (), s32[]{:S(2)}) async-start(), calls=%async_computation.5 | async-start | bytes 1802240 | tf_op jit(solution)/shard_map/all_gather | solution.py:36
  74.2 60.4 %copy-start.3 = (f32[256,704]{0,1:T(8,128)}, f32[256,704]{0,1:T(8,128)S(1)}, u32[]{:S(2)}) copy-start(f32[256,704]{0,1:T(8,128)S(1)} %fusion.8) | copy-start | bytes 2162692
  74.2 60.4 %copy-start.2 = (bf16[256,2048]{1,0:T(8,128)(2,1)S(1)}, bf16[256,2048]{1,0:T(8,128)(2,1)}, u32[]{:S(2)}) copy-start(bf16[256,2048]{1,0:T(8,128)(2,1)} %param.9) | copy-start | bytes 3145732
  134.6 146.2 %all-reduce.5.cloned.1.call-start = ((), (), s32[]{:S(2)}) async-start(), calls=%async_computation.6 | async-start | bytes 1441792 | tf_op jit(solution)/shard_map/psum | solution.py:37
  246.3 3.3 %copy-start.4 = (f32[256,704]{0,1:T(8,128)S(1)}, f32[256,704]{0,1:T(8,128)}, u32[]{:S(2)}) copy-start(f32[256,704]{0,1:T(8,128)} %copy-done.3) | copy-start | bytes 2162692
  249.5 70.4 %all-reduce.3.cloned.1.call-start = ((), (), s32[]{:S(2)}) async-start(), calls=%async_computation.4 | async-start | bytes 2097152 | tf_op jit(solution)/shard_map/psum | solution.py:34
  249.6 3.5 %copy-start.1 = (bf16[2048,704]{0,1:T(8,128)(2,1)S(1)}, bf16[2048,704]{0,1:T(8,128)(2,1)}, u32[]{:S(2)}) copy-start(bf16[2048,704]{0,1:T(8,128)(2,1)} %all-gather.7.cloned.1.call-done) | copy-start | bytes 8650756
  249.6 3.5 %copy-start.5 = (f32[256,704]{0,1:T(8,128)S(1)}, f32[256,704]{0,1:T(8,128)}, u32[]{:S(2)}) copy-start(f32[256,704]{0,1:T(8,128)} %fusion.7) | copy-start | bytes 2162692
Sparse Core Ops, SparseCore 0:
  9.6 61.8 all-gather.8
  73.0 57.7 all-gather.6
  132.4 77.6 all-gather.4
  211.6 34.6 all-gather.10
  249.6 31.1 all-reduce.4
  283.6 36.2 all-reduce.2
where the time goes:
time: 329 us
  waiting for transfers between devices  221 us (67%)
  blocking collectives  68.9 us (21%)
  matrix products  19.2 us (6%)
  between operations  14.2 us (4%)
  local copies, waits for them, and re-layouts  3.4 us (1%)
    all_gather x1, waiting for transfers between devices, on_device(): lax.all_gather(gate_weight, 'fs', axis=0, tiled=True)  62 us
    all_to_all x1, blocking collectives, on_device(): lax.all_to_all(out_grad, 'fs', split_axis=1, concat_axis=0, tiled=True)  56.6 us
    all_gather x1, waiting for transfers between devices, on_device(): lax.all_gather(up_weight, 'fs', axis=0, tiled=True)  56.6 us
    all_gather x1, waiting for transfers between devices, on_device(): lax.all_gather(hidden, 'fs', axis=0, tiled=True)  32.2 us
    psum x1, waiting for transfers between devices, on_device(): shard = lax.psum(shard.astype(jnp.bfloat16), 'rep').astype(jnp.float32)  25.6 us
    psum x1, waiting for transfers between devices, on_device(): input_grad = lax.psum(partial_value.astype(jnp.bfloat16), 'tp')  24.5 us
    all_gather x1, waiting for transfers between devices, on_device(): down_full = lax.all_gather(down_weight, 'fs', axis=1, tiled=True)  17.8 us
    psum x1, blocking collectives, on_device(): norms = lax.psum(jnp.sum(shard * shard, axis=1), 'fs')  12.2 us
  transfers between devices with their start and end apart: 6, of which 6 were waited for; matrix products, arithmetic and copies ran while one was open for 6% of the time, Pallas kernels for 0%

commit v1 on v0

--- a/solution.py
+++ b/solution.py
@@ -34,7 +34,7 @@
     input_grad = lax.psum(partial_value.astype(jnp.bfloat16), "tp")
     columns = lax.all_to_all(out_grad, "fs", split_axis=1, concat_axis=0, tiled=True)
     shard = contract_first(lax.all_gather(hidden, "fs", axis=0, tiled=True), columns)
-    shard = lax.psum(shard.astype(jnp.bfloat16), "rep").astype(jnp.float32)
+    shard = jnp.sum(lax.all_gather(shard.astype(jnp.bfloat16), "rep"), axis=0).astype(jnp.float32)
     norms = lax.psum(jnp.sum(shard * shard, axis=1), "fs")
     return (input_grad, shard, norms)
 

time: 329 us -> 322 us (0.979)
  blocking collectives: 68.9 us -> 62.6 us
  matrix products: 19.2 us -> 15.9 us
    all_gather x1, waiting for transfers between devices: 17.8 us -> 56.3 us  [on_device(): down_full = lax.all_gather(down_weight, 'fs', axis=1, tiled=True)]
    all_gather x1, waiting for transfers between devices: 32.2 us -> 0.83 us  [on_device(): lax.all_gather(hidden, 'fs', axis=0, tiled=True)]
    psum x1 -> x0, waiting for transfers between devices: 25.6 us -> none  [on_device(): shard = lax.psum(shard.astype(jnp.bfloat16), 'rep').astype(jnp.float32)]
    all_gather x0 -> x1, waiting for transfers between devices: none -> 19 us  [on_device(): lax.all_gather(shard.astype(jnp.bfloat16), 'rep')]
    all_to_all x1, blocking collectives: 56.6 us -> 50.3 us  [on_device(): lax.all_to_all(out_grad, 'fs', split_axis=1, concat_axis=0, tiled=True)]
    dot_general x3, matrix products: 9.5 us -> 6.15 us  [contract_last(): lax.dot_general(left, right, (((1,), (1,)), ((), ())), preferred_element_...]
  transfers between devices with their start and end apart: 6 -> 6, of which waited for: 6 -> 6; matrix products, arithmetic and copies ran while one was open for 6% -> 5% of each run, Pallas kernels for 0% -> 0%
where the time goes in v1:
time: 322 us; the launch traced here: 321 us
  waiting for transfers between devices  221 us (69%)
  blocking collectives  62.6 us (19%)
  matrix products  15.9 us (5%)
  between operations  14.2 us (4%)
  local copies, waits for them, and re-layouts  4.01 us (1%)
  other arithmetic  3.25 us (1%)
    all_gather x1, waiting for transfers between devices, on_device(): lax.all_gather(gate_weight, 'fs', axis=0, tiled=True)  62.7 us
    all_gather x1, waiting for transfers between devices, on_device(): lax.all_gather(up_weight, 'fs', axis=0, tiled=True)  56.6 us
    all_gather x1, waiting for transfers between devices, on_device(): down_full = lax.all_gather(down_weight, 'fs', axis=1, tiled=True)  56.3 us
    all_to_all x1, blocking collectives, on_device(): lax.all_to_all(out_grad, 'fs', split_axis=1, concat_axis=0, tiled=True)  50.3 us
    psum x1, waiting for transfers between devices, on_device(): input_grad = lax.psum(partial_value.astype(jnp.bfloat16), 'tp')  23.6 us
    all_gather x1, waiting for transfers between devices, on_device(): lax.all_gather(shard.astype(jnp.bfloat16), 'rep')  19 us
    psum x1, blocking collectives, on_device(): norms = lax.psum(jnp.sum(shard * shard, axis=1), 'fs')  12.2 us
  transfers between devices with their start and end apart: 6, of which 6 were waited for; matrix products, arithmetic and copies ran while one was open for 5% of the time, Pallas kernels for 0%

profile of v1, /device:TPU:0, one launch (start us, length us, event | category | flops | bytes accessed | tf_op | source)
XLA Modules:
  0.0 321.2 jit_solution(5377244753286905708)
XLA Ops:
  7.2 0.7 all-gather.11.cloned.1.call-update
  8.0 0.7 all-gather.9.cloned.1.call-update
  8.7 62.7 %all-gather.11.cloned.1.call-done = bf16[2048,704]{0,1:T(8,128)(2,1)} async-done(((bf16[512,704]{0,1:T(8,128)(2,1)}), bf16[2048,704]{0,1:T(8,128)(2,1)}) %all-gather.11.cloned.1.call-update) | async-done | bytes 2883600 | tf_op jit(solution)/shard_map/all_gather | solution.py:22
  71.4 2.8 fusion.8
  74.2 56.6 %all-gather.9.cloned.1.call-done = bf16[2048,704]{0,1:T(8,128)(2,1)} async-done(((bf16[512,704]{0,1:T(8,128)(2,1)}), bf16[2048,704]{0,1:T(8,128)(2,1)}) %all-gather.9.cloned.1.call-update) | async-done | bytes 2883600 | tf_op jit(solution)/shard_map/all_gather | solution.py:23
  130.8 3.8 %multiply_convert_fusion = (bf16[256,704]{0,1:T(8,128)(2,1)}, f32[256,704]{0,1:T(8,128)}) fusion(f32[256,704]{0,1:T(8,128)S(1)} %fusion.8, bf16[256,2048]{1,0:T(8,128)(2,1)S(1)} %copy-done, bf16[2048,704]{0,1:T(8,128)(2,1)} %all-gather.9.cloned.1.call-done), kind=kOutput, calls=%fused_computation.4 | convolution fusion | flops 739278848 | bytes 5734400 | tf_op jit(solution)/shard_map/dot_general | solution.py:26
  134.7 0.5 all-gather.7.cloned.1.call-update
  135.2 0.5 copy.8
  135.8 50.3 %all_to_all.19 = bf16[256,4,512]{0,2,1:T(8,128)(2,1)S(1)} all-to-all(bf16[256,4,512]{0,2,1:T(8,128)(2,1)S(1)} %bitcast.15), channel_id=1, replica_groups=mesh['rep'=2,'fs'=4,'tp'=4] {'fs'}, dimensions={1} | all-to-all | bytes 2097152 | tf_op jit(solution)/shard_map/all_to_all | solution.py:35
  186.1 0.5 copy.9
  186.6 0.8 all-gather.13.cloned.1.call-done
  187.5 3.2 %convolution_convert_fusion = bf16[704,512]{1,0:T(8,128)(2,1)} fusion(bf16[1024,704]{0,1:T(8,128)(2,1)} %all-gather.13.cloned.1.call-done, bf16[1024,512]{1,0:T(8,128)(2,1)S(1)} %bitcast.17), kind=kOutput, calls=%fused_computation.3 | convolution fusion | flops 738557952 | bytes 3211264 | tf_op jit(solution)/shard_map/dot_general | solution.py:14
  190.7 0.0 all-reduce.2.cloned.1.call-start
  190.8 56.3 %all-gather.7.cloned.1.call-done = bf16[704,2048]{1,0:T(8,128)(2,1)} async-done(((bf16[704,512]{1,0:T(8,128)(2,1)}), bf16[704,2048]{1,0:T(8,128)(2,1)}) %all-gather.7.cloned.1.call-update) | async-done | bytes 2883600 | tf_op jit(solution)/shard_map/all_gather | solution.py:20
  247.1 2.9 fusion.7
  250.1 1.2 fusion.2
  251.3 0.6 copy-done.1
  251.9 2.0 fusion
  254.0 19.0 %all-gather.15.cloned.1.call-done = bf16[1408,512]{1,0:T(8,128)(2,1)} async-done(((bf16[704,512]{1,0:T(8,128)(2,1)}), bf16[1408,512]{1,0:T(8,128)(2,1)}) %all-gather.15.cloned.1.call-update) | async-done | bytes 1441808 | tf_op jit(solution)/shard_map/all_gather | solution.py:37
  272.9 2.0 reduce_sum.21
  275.0 1.2 multiply_reduce_fusion
  276.2 12.2 %psum.15 = f32[704]{0:T(1024)} all-reduce(f32[704]{0:T(1024)S(1)} %get-tuple-element.3), channel_id=1, replica_groups=mesh['rep'=2,'fs'=4,'tp'=4] {'fs'}, use_global_device_ids=true, to_apply=%region_3.0 | all-reduce | flops 704 | bytes 5632 | tf_op jit(solution)/shard_map/psum | solution.py:38
  288.4 23.6 %all-reduce.2.cloned.1.call-done = bf16[256,2048]{1,0:T(8,128)(2,1)} async-done(((bf16[256,2048]{1,0:T(8,128)(2,1)}), bf16[256,2048]{1,0:T(8,128)(2,1)}) %all-reduce.2.cloned.1.call-update) | async-done | bytes 1048592 | tf_op jit(solution)/shard_map/psum | solution.py:34
  312.1 2.3 copy.11
  (23 shorter events, 0.3 us)
Async XLA Ops:
  7.2 64.3 %copy-start = (bf16[256,2048]{1,0:T(8,128)(2,1)S(1)}, bf16[256,2048]{1,0:T(8,128)(2,1)}, u32[]{:S(2)}) copy-start(bf16[256,2048]{1,0:T(8,128)(2,1)} %param.5) | copy-start | bytes 3145732
  7.2 64.2 %all-gather.11.cloned.1.call-start = ((), (), s32[]{:S(2)}) async-start(), calls=%async_computation.3 | async-start | bytes 3604480 | tf_op jit(solution)/shard_map/all_gather | solution.py:22
  7.9 122.9 %all-gather.9.cloned.1.call-start = ((), (), s32[]{:S(2)}) async-start(), calls=%async_computation.2 | async-start | bytes 3604480 | tf_op jit(solution)/shard_map/all_gather | solution.py:23
  8.7 178.8 %all-gather.13.cloned.1.call-start = ((), (), s32[]{:S(2)}) async-start(), calls=%async_computation.5 | async-start | bytes 1802240 | tf_op jit(solution)/shard_map/all_gather | solution.py:36
  74.2 60.4 %copy-start.4 = (f32[256,704]{0,1:T(8,128)}, f32[256,704]{0,1:T(8,128)S(1)}, u32[]{:S(2)}) copy-start(f32[256,704]{0,1:T(8,128)S(1)} %fusion.8) | copy-start | bytes 2162692
  74.2 61.0 %copy-start.2 = (bf16[256,2048]{1,0:T(8,128)(2,1)S(1)}, bf16[256,2048]{1,0:T(8,128)(2,1)}, u32[]{:S(2)}) copy-start(bf16[256,2048]{1,0:T(8,128)(2,1)} %param.9) | copy-start | bytes 3145732
  134.6 112.5 %all-gather.7.cloned.1.call-start = ((), (), s32[]{:S(2)}) async-start(), calls=%async_computation.1 | async-start | bytes 3604480 | tf_op jit(solution)/shard_map/all_gather | solution.py:20
  135.2 137.8 %all-gather.15.cloned.1.call-start = ((), (), s32[]{:S(2)}) async-start(), calls=%async_computation.6 | async-start | bytes 2162688 | tf_op jit(solution)/shard_map/all_gather | solution.py:37
  187.5 59.7 %copy-start.3 = (bf16[256,2048]{1,0:T(8,128)(2,1)S(1)}, bf16[256,2048]{1,0:T(8,128)(2,1)}, u32[]{:S(2)}) copy-start(bf16[256,2048]{1,0:T(8,128)(2,1)} %param.9) | copy-start | bytes 3145732
  190.7 59.4 %copy-start.5 = (f32[256,704]{0,1:T(8,128)S(1)}, f32[256,704]{0,1:T(8,128)}, u32[]{:S(2)}) copy-start(f32[256,704]{0,1:T(8,128)} %copy-done.4) | copy-start | bytes 2162692
  190.7 59.4 %copy-start.7 = (f32[256,704]{0,1:T(8,128)S(1)}, f32[256,704]{0,1:T(8,128)}, u32[]{:S(2)}) copy-start(f32[256,704]{0,1:T(8,128)} %get-tuple-element.6) | copy-start | bytes 2162692
  190.7 121.3 %all-reduce.2.cloned.1.call-start = ((), (), s32[]{:S(2)}) async-start(), calls=%async_computation.4 | async-start | bytes 2097152 | tf_op jit(solution)/shard_map/psum | solution.py:34
  247.1 2.9 copy-start.6
  250.1 1.8 copy-start.1
Sparse Core Ops, SparseCore 0:
  9.6 61.8 all-gather.10
  73.0 57.7 all-gather.8
  134.7 52.6 all-gather.12
  188.9 58.1 all-gather.6
  248.5 24.3 all-gather.14
  275.7 36.2 all-reduce.1
